TPU v7x, 256 devices: a 4x2x16 block of a 4x16x16 slice. The times are simulated.
256 devices in a mesh: grp: 2 (over y), fs: 32 (over z, core), tp: 4 (over x).
Axes of the slice: x: 4, y: 2, z: 16, core: 2. Of those that a mesh axis runs over, the one named last changes fastest.
The devices are a block of a 4x16x16 slice.
Arguments:
- tokens: bfloat16 [1536, 2048], P(('grp', 'tp')), parts along dimension 0, may hold values from -6 to 6
- norm_gain: float32 [2048], P('fs'), may hold values from 0.1 to 1.9
- up_trained: float32 [2048, 8192], P('fs', 'tp'), may hold values from -0.125 to 0.125
- down_trained: float32 [2048, 8192], P('fs', 'tp'), may hold values from -0.125 to 0.125
Outputs:
- up_serving: bfloat16 [4096, 8192], P('grp', 'fs'), parts along dimension 0
- down_serving: bfloat16 [4096, 8192], P('grp', 'fs'), parts along dimension 0
- prompt_output: bfloat16 [1536, 2048], P(('grp', 'tp'), 'fs'), parts along dimension 0
There are 2 independent parts, one for each index of `grp`. A program takes and returns all parts, laid end to end along the dimension named above; an argument that names none is the same for every part. Nothing has to cross between parts.
All inputs are finite; a program needn't handle non-finite values.
Results may differ from a plain program's by a relative error of at most 0.0074.
Values may be sent and summed in bfloat16 or wider, within the bound.
No kernel may reach another device: no remote copies, remote signals or barrier semaphores. Data moves between devices by JAX's collectives and lax.ppermute only.
A program may use at most 64 MiB of HBM per device.

v0:
```python
import jax
import jax.numpy as jnp
from jax import lax
from jax.sharding import PartitionSpec as P

epsilon = 1e-06


def joined_along(parts, dim):
    parts = jnp.moveaxis(parts, 0, dim)
    dims = parts.shape
    return parts.reshape(*dims[:dim], dims[dim] * dims[dim + 1], *dims[dim + 2 :])


def copy_for_each(x, axis):
    devices = lax.axis_size(axis)
    return lax.all_to_all(jnp.broadcast_to(x[None], (devices, *x.shape)), axis, 0, 0, tiled=True)


def collect(x, axis, dim):
    return joined_along(copy_for_each(x, axis), dim)


def in_blocks(x, dim, devices):
    dims = x.shape
    parts = x.reshape(*dims[:dim], devices, dims[dim] // devices, *dims[dim + 1 :])
    return jnp.moveaxis(parts, dim, 0)


def sum_at_owner(x, axis, dim):
    parts = in_blocks(x, dim, lax.axis_size(axis))
    arrived = lax.all_to_all(parts, axis, split_axis=0, concat_axis=0, tiled=True)
    return arrived.astype(jnp.float32).sum(axis=0)


def local(tokens, norm_gain, up_trained, down_trained):
    shards = lax.axis_size("fs")
    groups = lax.axis_size("tp")
    rows_local = up_trained.shape[0]
    cols_local = up_trained.shape[1]
    folded = (norm_gain[:, None] * up_trained).astype(jnp.bfloat16)
    stacked = jnp.stack([folded, down_trained.astype(jnp.bfloat16)])
    served_width = cols_local * groups // shards
    blocks_here = cols_local // served_width
    quarter_rows = rows_local // groups
    pieces = stacked.reshape(2, groups, quarter_rows, blocks_here, served_width)
    moved = lax.all_to_all(pieces, "tp", split_axis=1, concat_axis=3, tiled=True)
    placed = lax.all_to_all(moved, "fs", split_axis=3, concat_axis=2, tiled=True)
    ordered = placed.reshape(2, shards, quarter_rows, served_width)
    joined = collect(ordered, "tp", 2)
    owned = joined.reshape(2, rows_local * shards, served_width)
    up_serving = owned[0]
    down_serving = owned[1]
    values = tokens.astype(jnp.float32)
    scale = lax.rsqrt(jnp.mean(values * values, axis=1, keepdims=True) + epsilon)
    normed = (values * scale).astype(jnp.bfloat16)
    hidden = jnp.dot(normed, up_serving, preferred_element_type=jnp.float32)
    active = jnp.square(jax.nn.relu(hidden)).astype(jnp.bfloat16)
    summed = sum_at_owner(
        lax.dot_general(
            down_serving, active, (((1,), (1,)), ((), ())), preferred_element_type=jnp.float32
        ).astype(jnp.bfloat16),
        "fs",
        0,
    )
    prompt_output = summed.T.astype(jnp.bfloat16)
    return (up_serving, down_serving, prompt_output)


def solution(mesh):
    in_specs = (P(("grp", "tp"), None), P("fs"), P("fs", "tp"), P("fs", "tp"))
    out_specs = (P("grp", "fs"), P("grp", "fs"), P(("grp", "tp"), "fs"))
    return jax.shard_map(local, mesh=mesh, in_specs=in_specs, out_specs=out_specs, check_vma=False)
```

profile of v0, /device:TPU:33, one launch (start us, length us, event | category | flops | bytes accessed | tf_op | source)
XLA Modules:
  0.0 171.2 jit_solution(14890770866300171647)
XLA Ops:
  0.6 0.0 copy-start.3
  0.6 1.2 multiply_convert_fusion
  1.8 0.1 copy.23
  1.9 0.0 copy-done.3
  2.0 0.1 copy.24
  2.0 0.1 pad_maximum_fusion
  2.1 11.9 %all_to_all.43 = bf16[2,4,16,8,256]{4,3,2,0,1:T(8,128)(2,1)S(1)} all-to-all(bf16[2,4,16,8,256]{4,3,2,0,1:T(8,128)(2,1)S(1)} %copy.17), channel_id=1, replica_groups=mesh['grp'=2,'fs'=32,'tp'=4] {'tp'}, dimensions={1} | all-to-all | bytes 1048576 | tf_op jit(solution)/shard_map/all_to_all | solution.py:47
  14.0 0.1 copy.28
  14.0 0.3 copy.19
  14.3 60.6 %all_to_all.44 = bf16[2,1,16,32,256]{4,2,0,1,3:T(8,128)(2,1)S(1)} all-to-all(bf16[2,1,16,32,256]{4,2,0,1,3:T(8,128)(2,1)S(1)} %copy.19), channel_id=1, replica_groups=mesh['grp'=2,'fs'=32,'tp'=4] {'fs'}, dimensions={3} | all-to-all | bytes 1048576 | tf_op jit(solution)/shard_map/all_to_all | solution.py:48
  75.0 1.5 broadcast_in_dim.10
  76.5 3.8 %all-to-all-start.2 = ((bf16[4,2,32,16,256]{4,3,2,1,0:T(8,128)(2,1)}), bf16[4,2,32,16,256]{4,3,2,1,0:T(8,128)(2,1)S(1)}, u32[]{:S(2)}, u32[]{:S(2)}) async-start(bf16[4,2,32,16,256]{4,3,2,1,0:T(8,128)(2,1)} %broadcast_in_dim.10), calls=%async_computation.2 | async-start | bytes 4194304 | tf_op jit(solution)/shard_map/all_to_all | solution.py:17
  80.4 0.0 copy-done.2
  80.4 0.2 fusion
  80.6 25.6 %all-to-all-done.2 = bf16[4,2,32,16,256]{4,3,2,1,0:T(8,128)(2,1)S(1)} async-done(((bf16[4,2,32,16,256]{4,3,2,1,0:T(8,128)(2,1)}), bf16[4,2,32,16,256]{4,3,2,1,0:T(8,128)(2,1)S(1)}, u32[]{:S(2)}, u32[]{:S(2)}) %all-to-all-start.2) | async-done | bytes 2097184 | tf_op jit(solution)/shard_map/all_to_all | solution.py:17
  106.2 0.3 copy.27
  106.5 0.2 fusion.10
  106.8 0.0 copy-start.1
  106.8 0.0 copy-start
  106.8 0.9 copy-done.1
  107.7 2.3 %convolution_convert_fusion = bf16[2048,192]{0,1:T(8,128)(2,1)S(1)} fusion(bf16[2048,256]{1,0:T(8,128)(2,1)S(1)} %bitcast.29, bf16[2048,256]{1,0:T(8,128)(2,1)S(1)} %bitcast.31, bf16[192,2048]{1,0:T(8,128)(2,1)} %param.4, f32[192]{0:T(256)S(1)} %add_rsqrt_fusion), kind=kOutput, calls=%fused_computation | convolution fusion | flops 404373504 | bytes 3670784 | tf_op jit(solution)/shard_map/dot_general | solution.py:60
  110.0 0.5 copy.22
  110.5 59.9 %all_to_all.45 = bf16[32,64,192]{2,1,0:T(8,128)(2,1)S(1)} all-to-all(bf16[32,64,192]{2,1,0:T(8,128)(2,1)S(1)} %bitcast.28), channel_id=1, replica_groups=mesh['grp'=2,'fs'=32,'tp'=4] {'fs'}, dimensions={0} | all-to-all | bytes 1572864 | tf_op jit(solution)/shard_map/all_to_all | solution.py:32
  170.4 0.8 reduce_sum.22
  (6 shorter events, 0.1 us)
Async XLA Ops:
  0.6 1.3 copy-start.3
  76.5 3.8 %copy-start.2 = (bf16[192,2048]{1,0:T(8,128)(2,1)S(1)}, bf16[192,2048]{1,0:T(8,128)(2,1)}, u32[]{:S(2)}) copy-start(bf16[192,2048]{1,0:T(8,128)(2,1)} %param.4) | copy-start | bytes 2359300
  76.5 29.7 %all-to-all-start.2 = ((bf16[4,2,32,16,256]{4,3,2,1,0:T(8,128)(2,1)}), bf16[4,2,32,16,256]{4,3,2,1,0:T(8,128)(2,1)S(1)}, u32[]{:S(2)}, u32[]{:S(2)}) async-start(bf16[4,2,32,16,256]{4,3,2,1,0:T(8,128)(2,1)} %broadcast_in_dim.10), calls=%async_computation.2 | async-start | bytes 4194304 | tf_op jit(solution)/shard_map/all_to_all | solution.py:17
  106.8 1.0 copy-start.1
  106.8 3.3 %copy-start = (bf16[1,32,4,16,256]{4,3,2,1,0:T(8,128)(2,1)}, bf16[1,32,4,16,256]{4,3,2,1,0:T(8,128)(2,1)S(1)}, u32[]{:S(2)}) copy-start(bf16[1,32,4,16,256]{4,3,2,1,0:T(8,128)(2,1)S(1)} %get-tuple-element.3) | copy-start | bytes 3145732
where the time goes:
time: 172 us; the launch traced here: 171 us
  blocking collectives  132 us (77%)
  waiting for transfers between devices  25.6 us (15%)
  local copies, waits for them, and re-layouts  4.06 us (2%)
  starting transfers between devices  3.83 us (2%)
  other arithmetic  2.33 us (1%)
  matrix products  2.28 us (1%)
    all_to_all x1, blocking collectives, local(): lax.all_to_all(moved, 'fs', split_axis=3, concat_axis=2, tiled=True)  60.6 us
    all_to_all x1, blocking collectives, sum_at_owner(): lax.all_to_all(parts, axis, split_axis=0, concat_axis=0, tiled=True)  59.9 us
    all_to_all x1, waiting for transfers between devices, copy_for_each(): lax.all_to_all(jnp.broadcast_to(x[None], (devices, *x.shape)), axis, 0, 0...  25.6 us
    all_to_all x1, blocking collectives, local(): lax.all_to_all(pieces, 'tp', split_axis=1, concat_axis=3, tiled=True)  11.9 us
    all_to_all x1, starting transfers between devices, copy_for_each(): lax.all_to_all(jnp.broadcast_to(x[None], (devices, *x.shape)), axis, 0, 0...  3.83 us
  transfers between devices with their start and end apart: 1, of which 1 were waited for; matrix products, arithmetic and copies ran while one was open for 0% of the time, Pallas kernels for 0%

commit v1 on v0

--- a/solution.py
+++ b/solution.py
@@ -44,7 +44,9 @@
     blocks_here = cols_local // served_width
     quarter_rows = rows_local // groups
     pieces = stacked.reshape(2, groups, quarter_rows, blocks_here, served_width)
-    moved = lax.all_to_all(pieces, "tp", split_axis=1, concat_axis=3, tiled=True)
+    cells = jnp.split(pieces, lax.axis_size("tp"), axis=1)
+    incoming = lax.all_to_all(jnp.stack(cells), "tp", 0, 0)
+    moved = jnp.concatenate(incoming, axis=3)
     placed = lax.all_to_all(moved, "fs", split_axis=3, concat_axis=2, tiled=True)
     ordered = placed.reshape(2, shards, quarter_rows, served_width)
     joined = collect(ordered, "tp", 2)

time: 172 us -> 172 us (level)
  no operation moved by 1% of the time
where the time goes in v1:
time: 172 us; the launch traced here: 171 us
  blocking collectives  132 us (77%)
  waiting for transfers between devices  25.6 us (15%)
  local copies, waits for them, and re-layouts  4.1 us (2%)
  starting transfers between devices  3.83 us (2%)
  other arithmetic  2.35 us (1%)
  matrix products  2.28 us (1%)
    all_to_all x1, blocking collectives, local(): lax.all_to_all(moved, 'fs', split_axis=3, concat_axis=2, tiled=True)  60.6 us
    all_to_all x1, blocking collectives, sum_at_owner(): lax.all_to_all(parts, axis, split_axis=0, concat_axis=0, tiled=True)  59.9 us
    all_to_all x1, waiting for transfers between devices, copy_for_each(): lax.all_to_all(jnp.broadcast_to(x[None], (devices, *x.shape)), axis, 0, 0...  25.6 us
    all_to_all x1, blocking collectives, local(): incoming = lax.all_to_all(jnp.stack(cells), 'tp', 0, 0)  11.9 us
    all_to_all x1, starting transfers between devices, copy_for_each(): lax.all_to_all(jnp.broadcast_to(x[None], (devices, *x.shape)), axis, 0, 0...  3.83 us
  transfers between devices with their start and end apart: 1, of which 1 were waited for; matrix products, arithmetic and copies ran while one was open for 0% of the time, Pallas kernels for 0%

profile of v1, /device:TPU:33, one launch (start us, length us, event | category | flops | bytes accessed | tf_op | source)
XLA Modules:
  0.0 171.3 jit_solution(8238245732470622239)
XLA Ops:
  0.6 0.0 copy-start.3
  0.6 1.2 multiply_convert_fusion
  1.8 0.1 copy.24
  1.9 0.0 copy-done.3
  2.0 0.1 copy.25
  2.1 0.1 pad_maximum_fusion
  2.2 11.9 %all_to_all.30 = bf16[4,2,1,16,8,256]{5,4,3,1,2,0:T(8,128)(2,1)S(1)} all-to-all(bf16[4,2,1,16,8,256]{5,4,3,1,2,0:T(8,128)(2,1)S(1)} %pad_maximum_fusion), channel_id=1, replica_groups=mesh['grp'=2,'fs'=32,'tp'=4] {'tp'}, dimensions={0} | all-to-all | bytes 1048576 | tf_op jit(solution)/shard_map/all_to_all | solution.py:48
  14.0 0.1 copy.29
  14.1 0.3 copy.20
  14.4 60.6 %all_to_all.31 = bf16[2,1,16,32,256]{4,2,0,1,3:T(8,128)(2,1)S(1)} all-to-all(bf16[2,1,16,32,256]{4,2,0,1,3:T(8,128)(2,1)S(1)} %copy.20), channel_id=1, replica_groups=mesh['grp'=2,'fs'=32,'tp'=4] {'fs'}, dimensions={3} | all-to-all | bytes 1048576 | tf_op jit(solution)/shard_map/all_to_all | solution.py:50
  75.1 1.5 broadcast_in_dim.10
  76.6 3.8 %all-to-all-start.2 = ((bf16[4,2,32,16,256]{4,3,2,1,0:T(8,128)(2,1)}), bf16[4,2,32,16,256]{4,3,2,1,0:T(8,128)(2,1)S(1)}, u32[]{:S(2)}, u32[]{:S(2)}) async-start(bf16[4,2,32,16,256]{4,3,2,1,0:T(8,128)(2,1)} %broadcast_in_dim.10), calls=%async_computation.2 | async-start | bytes 4194304 | tf_op jit(solution)/shard_map/all_to_all | solution.py:17
  80.4 0.0 copy-done.2
  80.4 0.2 fusion
  80.7 25.6 %all-to-all-done.2 = bf16[4,2,32,16,256]{4,3,2,1,0:T(8,128)(2,1)S(1)} async-done(((bf16[4,2,32,16,256]{4,3,2,1,0:T(8,128)(2,1)}), bf16[4,2,32,16,256]{4,3,2,1,0:T(8,128)(2,1)S(1)}, u32[]{:S(2)}, u32[]{:S(2)}) %all-to-all-start.2) | async-done | bytes 2097184 | tf_op jit(solution)/shard_map/all_to_all | solution.py:17
  106.3 0.3 copy.28
  106.6 0.2 fusion.10
  106.8 0.0 copy-start.1
  106.8 0.0 copy-start
  106.8 0.9 copy-done.1
  107.8 2.3 %convolution_convert_fusion = bf16[2048,192]{0,1:T(8,128)(2,1)S(1)} fusion(bf16[2048,256]{1,0:T(8,128)(2,1)S(1)} %bitcast.37, bf16[2048,256]{1,0:T(8,128)(2,1)S(1)} %bitcast.39, bf16[192,2048]{1,0:T(8,128)(2,1)} %param.4, f32[192]{0:T(256)S(1)} %add_rsqrt_fusion), kind=kOutput, calls=%fused_computation | convolution fusion | flops 404373504 | bytes 3670784 | tf_op jit(solution)/shard_map/dot_general | solution.py:62
  110.1 0.5 copy.23
  110.6 59.9 %all_to_all.32 = bf16[32,64,192]{2,1,0:T(8,128)(2,1)S(1)} all-to-all(bf16[32,64,192]{2,1,0:T(8,128)(2,1)S(1)} %bitcast.36), channel_id=1, replica_groups=mesh['grp'=2,'fs'=32,'tp'=4] {'fs'}, dimensions={0} | all-to-all | bytes 1572864 | tf_op jit(solution)/shard_map/all_to_all | solution.py:32
  170.5 0.8 reduce_sum.22
  (8 shorter events, 0.2 us)
Async XLA Ops:
  0.6 1.3 copy-start.3
  76.6 3.8 %copy-start.2 = (bf16[192,2048]{1,0:T(8,128)(2,1)S(1)}, bf16[192,2048]{1,0:T(8,128)(2,1)}, u32[]{:S(2)}) copy-start(bf16[192,2048]{1,0:T(8,128)(2,1)} %param.4) | copy-start | bytes 2359300
  76.6 29.7 %all-to-all-start.2 = ((bf16[4,2,32,16,256]{4,3,2,1,0:T(8,128)(2,1)}), bf16[4,2,32,16,256]{4,3,2,1,0:T(8,128)(2,1)S(1)}, u32[]{:S(2)}, u32[]{:S(2)}) async-start(bf16[4,2,32,16,256]{4,3,2,1,0:T(8,128)(2,1)} %broadcast_in_dim.10), calls=%async_computation.2 | async-start | bytes 4194304 | tf_op jit(solution)/shard_map/all_to_all | solution.py:17
  106.8 1.0 copy-start.1
  106.8 3.3 %copy-start = (bf16[1,32,4,16,256]{4,3,2,1,0:T(8,128)(2,1)}, bf16[1,32,4,16,256]{4,3,2,1,0:T(8,128)(2,1)S(1)}, u32[]{:S(2)}) copy-start(bf16[1,32,4,16,256]{4,3,2,1,0:T(8,128)(2,1)S(1)} %get-tuple-element.3) | copy-start | bytes 3145732
